TPU v7x, 32 devices: a whole 2x2x4 slice. The times are simulated.
32 devices in a mesh: sp: 16 (over z, y, x), tp: 2 (over core).
Axes of the slice: x: 2, y: 2, z: 4, core: 2. Of those that a mesh axis runs over, the one named last changes fastest.
Arguments:
- out_grad: bfloat16 [3584, 2048], P('sp'), may hold values from -6 to 6
- moe_input: bfloat16 [3584, 2048], P('sp'), may hold values from -6 to 6
- routes: int32 [3584, 2], P('sp'), may hold values from 0 to 15, all different within a row; in each aligned block of 224 rows (0 to 223, 224 to 447, ...) at most 56 rows name the same one
- route_weights: float32 [3584, 2], P('sp'), may hold values from 0.2 to 1
- conv_result: bfloat16 [3584, 1024], P('sp', 'tp'), may hold values from -60 to 60
- glu_value: bfloat16 [3584, 1024], P('sp', 'tp'), may hold values from -6 to 6
- glu_gate: bfloat16 [3584, 1024], P('sp', 'tp'), may hold values from -6 to 6
- conv_taps: bfloat16 [31, 1024], P(None, 'tp'), may hold values from -1 to 1
- norm_gain: float32 [1024], P('tp'), may hold values from 0.1 to 1.9
- proj_weight: bfloat16 [2048, 1024], P(None, 'tp'), may hold values from -0.1875 to 0.1875
- expert_gate: bfloat16 [16, 2048, 1024], P('sp', None, 'tp'), may hold values from -0.125 to 0.125
- expert_up: bfloat16 [16, 2048, 1024], P('sp', None, 'tp'), may hold values from -0.125 to 0.125
- expert_down: bfloat16 [16, 1024, 2048], P('sp', 'tp'), may hold values from -0.1875 to 0.1875
Outputs:
- input_grad: bfloat16 [3584, 2048], P('sp')
- proj_grad: float32 [2048, 1024], P('sp', 'tp')
- gate_grad: float32 [16, 2048, 1024], P('sp', None, 'tp')
- up_grad: float32 [16, 2048, 1024], P('sp', None, 'tp')
- down_grad: float32 [16, 1024, 2048], P('sp', 'tp')
- value_grad: bfloat16 [3584, 1024], P('sp', 'tp')
- gate_side_grad: bfloat16 [3584, 1024], P('sp', 'tp')
Inputs may be any that keep to these rules, and one draw needn't show every extreme that they name: `routes`: in each aligned block of 224 tokens no expert is named more than 56 times, a bound that some block reaches; a token's experts differ.
All inputs are finite; a program needn't handle non-finite values.
Results may differ from a plain program's by a relative error of at most 0.0061.
Values may be sent and summed in bfloat16 or wider, within the bound.
A program may use at most 128 MiB of HBM per device.

v0:
```python
import functools

import jax
import jax.numpy as jnp
from jax import lax
from jax.experimental import pallas as pl
from jax.experimental.pallas import tpu as pltpu
from jax.sharding import PartitionSpec as P

norm_eps = 1e-05
MESH = pl.DeviceIdType.MESH


def from_behind(shard, axis, by):
    count = lax.axis_size(axis)
    pairs = [(i, i + by) for i in range(count) if 0 <= i + by < count]
    return lax.ppermute(shard, axis, pairs)


def contract_rows(left, right):
    return lax.dot_general(
        left, right, (((0,), (0,)), ((), ())), preferred_element_type=jnp.float32
    )


def contract_cols(left, right):
    return lax.dot_general(
        left, right, (((1,), (1,)), ((), ())), preferred_element_type=jnp.float32
    )


def exchange_body(n, number, relay, lanes, *refs):
    xs, outs = refs[:number], refs[number : 2 * number]
    own_sem, send_sem, recv_sem = refs[2 * number : 2 * number + 3]
    fwd_send, fwd_recv = refs[2 * number + 3 :] if relay else (None, None)
    me = lax.axis_index("sp")
    half = lax.axis_index("tp")
    other = 1 - half

    def place(a, source, side):
        if not relay:
            return outs[a].at[source]
        if lanes:
            cols = xs[a].shape[2]
            return outs[a].at[source, :, pl.ds(pl.multiple_of(side * cols, cols), cols)]
        return outs[a].at[side, source]

    def outgoing(a, step):
        peer = lax.rem(me + step, n)
        return pltpu.make_async_remote_copy(
            src_ref=xs[a].at[peer],
            dst_ref=place(a, me, half),
            send_sem=send_sem.at[a, step],
            recv_sem=recv_sem.at[a, step],
            device_id=(peer, half),
            device_id_type=MESH,
        )

    def incoming(a, step):
        peer = lax.rem(me + step, n)
        source = lax.rem(me + n - step, n)
        return pltpu.make_async_remote_copy(
            src_ref=xs[a].at[peer],
            dst_ref=place(a, source, half),
            send_sem=send_sem.at[a, step],
            recv_sem=recv_sem.at[a, step],
            device_id=(peer, half),
            device_id_type=MESH,
        )

    def relayed(a, step, first=False):
        source = lax.rem(me + n - step, n)
        return pltpu.make_async_remote_copy(
            src_ref=xs[a].at[me] if first else place(a, source, half),
            dst_ref=place(a, source, half),
            send_sem=fwd_send.at[a, step],
            recv_sem=fwd_recv.at[a, step],
            device_id=(me, other),
            device_id_type=MESH,
        )

    def from_other(a, step):
        source = lax.rem(me + n - step, n)
        return pltpu.make_async_remote_copy(
            src_ref=xs[a].at[me],
            dst_ref=place(a, source, other),
            send_sem=fwd_send.at[a, step],
            recv_sem=fwd_recv.at[a, step],
            device_id=(me, other),
            device_id_type=MESH,
        )

    barrier = pltpu.get_barrier_semaphore()

    def greet(step, carry):
        pl.semaphore_signal(
            barrier, inc=1, device_id=(lax.rem(me + step, n), half), device_id_type=MESH
        )
        return carry

    lax.fori_loop(1, n, greet, 0)
    if relay:
        pl.semaphore_signal(barrier, inc=1, device_id=(me, other), device_id_type=MESH)
    pl.semaphore_wait(barrier, n - 1 + (1 if relay else 0))

    for a in range(number):

        def send(step, carry, a=a):
            outgoing(a, step).start()
            return carry

        lax.fori_loop(1, n, send, 0)
    own = []
    for a in range(number):
        own.append(pltpu.make_async_copy(xs[a].at[me], place(a, me, half), own_sem.at[a]))
        own[-1].start()
        if relay:
            relayed(a, 0, first=True).start()
    for a in range(number):

        def arrive(step, carry, a=a):
            incoming(a, step).wait_recv()
            if relay:
                relayed(a, step).start()
            return carry

        lax.fori_loop(1, n, arrive, 0)
    for a in range(number):

        def finish(step, carry, a=a):
            outgoing(a, step).wait_send()
            if relay:
                relayed(a, step).wait_send()
                from_other(a, step).wait_recv()
            return carry

        lax.fori_loop(1, n, finish, 0)
        own[a].wait()
        if relay:
            relayed(a, 0, first=True).wait_send()
            from_other(a, 0).wait_recv()


def exchange(arrays, collective_id, relay=True, lanes=True):
    n = lax.axis_size("sp")
    number = len(arrays)
    outs = []
    for x in arrays:
        shape = x.shape
        if relay:
            shape = (shape[0], shape[1], 2 * shape[2]) if lanes else (2,) + shape
        outs.append(jax.ShapeDtypeStruct(shape, x.dtype))
    sems = [pltpu.SemaphoreType.DMA((number,))] + [pltpu.SemaphoreType.DMA((number, n))] * (
        4 if relay else 2
    )
    return pl.pallas_call(
        functools.partial(exchange_body, n, number, relay, lanes),
        out_shape=tuple(outs),
        in_specs=[pl.BlockSpec(memory_space=pltpu.VMEM)] * number,
        out_specs=tuple([pl.BlockSpec(memory_space=pl.ANY)] * number),
        scratch_shapes=sems,
        compiler_params=pltpu.CompilerParams(collective_id=collective_id, has_side_effects=True),
    )(*arrays)


def per_device(
    out_grad,
    moe_input,
    routes,
    route_weights,
    conv_result,
    glu_value,
    glu_gate,
    conv_taps,
    norm_gain,
    proj_weight,
    expert_gate,
    expert_up,
    expert_down,
):
    n_sp = lax.axis_size("sp")
    n_tp = lax.axis_size("tp")
    half = lax.axis_index("tp")
    tok_rows, width = out_grad.shape
    top_count = routes.shape[1]
    capacity = 2 * top_count * tok_rows // n_sp
    slots = n_sp * capacity
    share = width // n_tp
    experts = jnp.arange(n_sp, dtype=jnp.int32)[None, :]
    named = [(routes[:, k : k + 1] == experts) for k in range(top_count)]
    per_token = sum(hit.astype(jnp.bfloat16) for hit in named)
    order = jnp.arange(tok_rows, dtype=jnp.int32)
    before = (order[None, :] < order[:, None]).astype(jnp.bfloat16)
    earlier = jnp.dot(before, per_token, preferred_element_type=jnp.float32).astype(jnp.int32)
    rows = jnp.arange(slots, dtype=jnp.int32)
    chosen = []
    for k in range(top_count):
        slot = jnp.sum(jnp.where(named[k], earlier, 0), axis=1)
        target = routes[:, k] * capacity + slot
        chosen.append(rows[:, None] == target[None, :])
    pick = functools.reduce(jnp.logical_or, chosen).astype(jnp.bfloat16)
    row_weight = sum(
        jnp.sum(jnp.where(chosen[k], route_weights[:, k][None, :], 0.0), axis=1)
        for k in range(top_count)
    )
    input_half = lax.dynamic_slice_in_dim(moe_input, half * share, share, 1)
    grad_half = lax.dynamic_slice_in_dim(out_grad, half * share, share, 1)
    send_input = jnp.dot(pick, input_half, preferred_element_type=jnp.float32).astype(jnp.bfloat16)
    send_grad = (
        jnp.dot(pick, grad_half, preferred_element_type=jnp.float32) * row_weight[:, None]
    ).astype(jnp.bfloat16)
    row_scale = float(slots) ** (-0.5)
    blocks = (n_sp, capacity, share)
    inputs, grads = exchange([send_input.reshape(blocks), send_grad.reshape(blocks)], 1)
    inputs, grads = inputs.reshape(slots, width), grads.reshape(slots, width)

    values = conv_result.astype(jnp.float32)
    channels = conv_result.shape[1] * n_tp
    sums, squares = lax.psum((jnp.sum(values, axis=1), jnp.sum(values * values, axis=1)), "tp")
    center = sums / channels
    spread = squares / channels - center * center
    inv_std = lax.rsqrt(spread + norm_eps)[:, None]
    normed = (values - center[:, None]) * inv_std
    scaled = normed * norm_gain[None, :]
    sig_norm = jax.nn.sigmoid(scaled)
    activ = (scaled * sig_norm).astype(jnp.bfloat16)
    all_activ = lax.all_gather(activ, "sp", axis=0, tiled=True)

    gate_pre = jnp.dot(inputs, expert_gate[0], preferred_element_type=jnp.float32)
    up_pre = jnp.dot(inputs, expert_up[0], preferred_element_type=jnp.float32)
    sigma = jax.nn.sigmoid(gate_pre)
    silu_gate = gate_pre * sigma
    hidden = (silu_gate * up_pre).astype(jnp.bfloat16)
    down_g = contract_rows(hidden, grads) * row_scale
    hidden_grad = contract_cols(grads, expert_down[0])
    gate_back = (hidden_grad * up_pre * sigma * (1.0 + gate_pre * (1.0 - sigma))).astype(
        jnp.bfloat16
    )
    up_back = (hidden_grad * silu_gate).astype(jnp.bfloat16)
    gate_g = contract_rows(inputs, gate_back) * row_scale
    up_g = contract_rows(inputs, up_back) * row_scale

    def partial_of(side):
        weight_g = lax.dynamic_slice_in_dim(expert_gate[0], side * share, share, 0)
        weight_u = lax.dynamic_slice_in_dim(expert_up[0], side * share, share, 0)
        return (contract_cols(gate_back, weight_g) + contract_cols(up_back, weight_u)).astype(
            jnp.bfloat16
        )

    arrived = lax.ppermute(
        partial_of(1 - half), "tp", [(i, n_tp - 1 - i) for i in range(n_tp)]
    )
    summed = (partial_of(half).astype(jnp.float32) + arrived.astype(jnp.float32)).astype(
        jnp.bfloat16
    )
    (returned,) = exchange([summed.reshape(blocks)], 2, relay=False)
    returned = returned.reshape(slots, share)
    grad_share = (grad_half.astype(jnp.float32) + contract_rows(pick, returned)).astype(
        jnp.bfloat16
    )
    input_grad = lax.all_gather(grad_share, "tp", axis=1, tiled=True)

    act_grad = jnp.dot(input_grad, proj_weight, preferred_element_type=jnp.float32)
    part = tok_rows // n_tp
    mine = lax.dynamic_slice_in_dim(input_grad, half * part, part, 0)
    mine = mine.reshape(part, n_sp, width // n_sp).transpose(1, 0, 2)
    (features,) = exchange([mine], 3, lanes=False)
    features = features.transpose(1, 0, 2, 3).reshape(n_sp * tok_rows, width // n_sp)
    token_scale = float(tok_rows * n_sp) ** (-0.5)
    proj_grad = contract_rows(features, all_activ) * token_scale

    norm_grad = act_grad * sig_norm * (1.0 + scaled * (1.0 - sig_norm)) * norm_gain[None, :]
    first, second = lax.psum(
        (jnp.sum(norm_grad, axis=1), jnp.sum(norm_grad * normed, axis=1)), "tp"
    )
    conv_grad = inv_std * (
        norm_grad - first[:, None] / channels - normed * (second[:, None] / channels)
    )
    reach = conv_taps.shape[0]
    rim = from_behind(conv_grad[: reach - 1].astype(jnp.bfloat16), "sp", -1).astype(jnp.float32)
    extended = jnp.concatenate([conv_grad, rim], axis=0)
    taps_float = conv_taps.astype(jnp.float32)
    mixed_grad = jnp.zeros_like(conv_grad)
    for lag in range(reach):
        mixed_grad = (
            mixed_grad + taps_float[reach - 1 - lag][None, :] * extended[lag : lag + tok_rows]
        )
    sig_gate = jax.nn.sigmoid(glu_gate.astype(jnp.float32))
    value_grad = (mixed_grad * sig_gate).astype(jnp.bfloat16)
    gate_side_grad = (
        mixed_grad * glu_value.astype(jnp.float32) * sig_gate * (1.0 - sig_gate)
    ).astype(jnp.bfloat16)
    return (
        input_grad,
        proj_grad,
        gate_g[None],
        up_g[None],
        down_g[None],
        value_grad,
        gate_side_grad,
    )


def solution(mesh):
    in_specs = (
        P("sp", None),
        P("sp", None),
        P("sp", None),
        P("sp", None),
        P("sp", "tp"),
        P("sp", "tp"),
        P("sp", "tp"),
        P(None, "tp"),
        P("tp"),
        P(None, "tp"),
        P("sp", None, "tp"),
        P("sp", None, "tp"),
        P("sp", "tp", None),
    )
    out_specs = (
        P("sp", None),
        P("sp", "tp"),
        P("sp", None, "tp"),
        P("sp", None, "tp"),
        P("sp", "tp", None),
        P("sp", "tp"),
        P("sp", "tp"),
    )
    return jax.shard_map(
        per_device, mesh=mesh, in_specs=in_specs, out_specs=out_specs, check_vma=False
    )
```

profile of v0, /device:TPU:14, one launch (start us, length us, event | category | flops | bytes accessed | tf_op | source)
XLA Modules:
  0.0 283.9 jit_solution(6806697640445566975)
XLA Ops:
  9.4 3.0 %convolution_convert_fusion = bf16[896,1024]{1,0:T(8,128)(2,1)} fusion(bf16[224,2048]{1,0:T(8,128)(2,1)} %param.14, s32[]{:T(128)S(6)} %select_n.27, s32[224]{0:T(256)S(1)} %get-tuple-element.65, s32[224]{0:T(256)S(1)} %get-tuple-element.66), kind=kOutput, calls=%fused_computation.47 | convolution fusion | flops 412561408 | bytes 2295556 | tf_op jit(solution)/shard_map/dot_general | solution.py:208
  12.5 2.0 multiply_convert_fusion
  14.5 91.7 %shard_map.180 = (bf16[16,56,2048]{2,1,0:T(8,128)(2,1)}, bf16[16,56,2048]{2,1,0:T(8,128)(2,1)}) custom-call(bf16[16,56,1024]{2,1,0:T(8,128)(2,1)} %bitcast.97, bf16[16,56,1024]{2,1,0:T(8,128)(2,1)} %bitcast.100), custom_call_target="tpu_custom_call" | custom-call | tf_op jit(solution)/shard_map/pallas_call | solution.py:156
  106.2 5.5 %fusion = f32[896,512]{1,0:T(8,128)} fusion(bf16[896,2048]{1,0:T(8,128)(2,1)} %bitcast.141, bf16[1,2048,512]{2,1,0:T(8,128)(2,1)S(1)} %copy-done), kind=kOutput, calls=%fused_computation.36 | convolution fusion | flops 1879048192 | bytes 7602176 | tf_op jit(solution)/shard_map/dot_general | solution.py:229
  111.7 3.3 %fusion.2 = f32[896,512]{1,0:T(8,128)} fusion(bf16[896,2048]{1,0:T(8,128)(2,1)S(1)} %bitcast.143, bf16[1,2048,512]{2,1,0:T(8,128)(2,1)S(1)} %copy-done.5), kind=kOutput, calls=%fused_computation.38 | convolution fusion | flops 1879048192 | bytes 7602176 | tf_op jit(solution)/shard_map/dot_general | solution.py:230
  115.0 6.4 %multiply_convert_fusion.2 = (bf16[896,512]{1,0:T(8,128)(2,1)S(1)}, bf16[896,512]{1,0:T(8,128)(2,1)S(1)}) fusion(f32[896,512]{1,0:T(8,128)} %fusion, f32[896,512]{1,0:T(8,128)} %fusion.2, bf16[896,2048]{1,0:T(8,128)(2,1)} %bitcast.139, bf16[1,512,2048]{2,1,0:T(8,128)(2,1)} %param.25), kind=kOutput, calls=%fused_computation.43 | convolution fusion | flops 1885011968 | bytes 11272192 | tf_op jit(solution)/shard_map/dot_general | solution.py:27
  123.3 2.4 add_convert_fusion.1
  126.3 3.6 %all-reduce.1 = (f32[224]{0:T(256)S(1)}, f32[224]{0:T(256)S(1)}) all-reduce(f32[224]{0:T(256)S(1)} %get-tuple-element.14, f32[224]{0:T(256)S(1)} %get-tuple-element.13), channel_id=1, replica_groups=mesh['sp'=16,'tp'=2] {'tp'}, use_global_device_ids=true, to_apply=%region_7.8 | all-reduce | flops 448 | bytes 3584 | tf_op jit(solution)/shard_map/psum | solution.py:219
  131.8 4.0 %add_convert_fusion = bf16[896,1024]{1,0:T(8,128)(2,1)} fusion(bf16[896,1024]{1,0:T(8,128)(2,1)} %collective-permute-done, f32[896,1024]{1,0:T(8,128)S(1)} %fusion.14, bf16[896,512]{1,0:T(8,128)(2,1)S(1)} %copy-done.4, bf16[1,2048,512]{2,1,0:T(8,128)(2,1)S(1)} %copy-done.7, s32[]{:T(128)S(6)} %select_n.27), kind=kOutput, calls=%fused_computation.32 | convolution fusion | flops 945029120 | bytes 9306116 | tf_op jit(solution)/shard_map/dot_general | solution.py:27
  135.7 48.7 %shard_map.181 = bf16[16,56,1024]{2,1,0:T(8,128)(2,1)} custom-call(bf16[16,56,1024]{2,1,0:T(8,128)(2,1)} %bitcast.96), custom_call_target="tpu_custom_call" | custom-call | tf_op jit(solution)/shard_map/pallas_call | solution.py:156
  184.5 2.4 fusion.7
  186.9 2.6 all_gather.6
  189.5 1.5 fusion.152
  191.0 2.4 all-reduce
  193.5 2.1 fusion.126
  196.9 6.8 %multiply_bitcast_fusion.1 = f32[1,2048,512]{2,1,0:T(8,128)} fusion(bf16[896,2048]{1,0:T(8,128)(2,1)} %bitcast.142, bf16[896,512]{1,0:T(8,128)(2,1)} %copy-done.3), kind=kOutput, calls=%fused_computation.30 | convolution fusion | flops 1880096768 | bytes 8781824 | tf_op jit(solution)/shard_map/dot_general | solution.py:21
  203.8 4.5 %multiply_bitcast_fusion.2 = f32[1,2048,512]{2,1,0:T(8,128)} fusion(bf16[896,2048]{1,0:T(8,128)(2,1)S(1)} %bitcast.144, bf16[896,512]{1,0:T(8,128)(2,1)S(1)} %get-tuple-element.24), kind=kOutput, calls=%fused_computation.31 | convolution fusion | flops 1880096768 | bytes 8781824 | tf_op jit(solution)/shard_map/dot_general | solution.py:21
  208.3 4.5 %multiply_bitcast_fusion = f32[1,512,2048]{2,1,0:T(8,128)} fusion(bf16[896,2048]{1,0:T(8,128)(2,1)S(1)} %bitcast.140, f32[896,512]{1,0:T(8,128)S(1)} %copy-done.19, f32[896,512]{1,0:T(8,128)S(1)} %copy-done.18), kind=kOutput, calls=%fused_computation.29 | convolution fusion | flops 1882849280 | bytes 11534336 | tf_op jit(solution)/shard_map/dot_general | solution.py:21
  212.8 1.9 collective-permute-start.1
  215.6 27.3 %shard_map.182 = bf16[2,16,112,128]{3,2,1,0:T(8,128)(2,1)} custom-call(bf16[16,112,128]{2,1,0:T(8,128)(2,1)} %bitcast_bitcast_fusion.refs_0_), custom_call_target="tpu_custom_call" | custom-call | tf_op jit(solution)/shard_map/pallas_call | solution.py:156
  243.0 2.2 copy.23
  245.2 4.0 %multiply_convert_fusion.5 = (bf16[224,512]{1,0:T(8,128)(2,1)}, f32[224,512]{1,0:T(8,128)S(1)}) fusion(bf16[224,512]{1,0:T(8,128)(2,1)S(1)} %copy-done.10, bf16[224,512]{1,0:T(8,128)(2,1)S(1)} %copy-done.8, f32[30,512]{1,0:T(8,128)S(1)} %convert_element_type.90, f32[224,512]{1,0:T(8,128)S(1)} %get-tuple-element.25, f32[512]{0:T(512)} %bitcast.113, ...), kind=kLoop, calls=%fused_computation.209 | loop fusion | flops 11583488 | bytes 1730560 | tf_op jit(solution)/shard_map/convert_element_type | solution.py:292
  250.0 22.5 %all-gather.2.cloned.1.call-done = bf16[3584,512]{1,0:T(8,128)(2,1)} async-done(((bf16[224,512]{1,0:T(8,128)(2,1)}), bf16[3584,512]{1,0:T(8,128)(2,1)}) %all-gather.2.cloned.1.call-update) | async-done | bytes 3670032 | tf_op jit(solution)/shard_map/all_gather | solution.py:227
  272.5 3.7 %convolution_multiply_fusion.1 = f32[128,512]{1,0:T(8,128)} fusion(bf16[3584,128]{1,0:T(8,128)(2,1)} %bitcast.98, bf16[3584,512]{1,0:T(8,128)(2,1)} %all-gather.2.cloned.1.call-done), kind=kOutput, calls=%fused_computation.53 | convolution fusion | flops 469827584 | bytes 4849664 | tf_op jit(solution)/shard_map/dot_general | solution.py:21
  (65 shorter events, 10.5 us)
Async XLA Ops:
  7.2 99.0 %copy-start = (bf16[1,2048,512]{2,1,0:T(8,128)(2,1)S(1)}, bf16[1,2048,512]{2,1,0:T(8,128)(2,1)}, u32[]{:S(2)}) copy-start(bf16[1,2048,512]{2,1,0:T(8,128)(2,1)} %param.23) | copy-start | bytes 6291460
  7.2 5.3 %copy-start.17 = (bf16[224,2048]{1,0:T(8,128)(2,1)S(1)}, bf16[224,2048]{1,0:T(8,128)(2,1)}, u32[]{:S(2)}) copy-start(bf16[224,2048]{1,0:T(8,128)(2,1)} %param.13) | copy-start | bytes 2752516
  7.2 265.3 %all-gather.2.cloned.1.call-start = ((), (), s32[]{:S(2)}) async-start(), calls=%async_computation | async-start | bytes 3899392 | tf_op jit(solution)/shard_map/all_gather | solution.py:227
  106.2 5.5 %copy-start.5 = (bf16[1,2048,512]{2,1,0:T(8,128)(2,1)S(1)}, bf16[1,2048,512]{2,1,0:T(8,128)(2,1)}, u32[]{:S(2)}) copy-start(bf16[1,2048,512]{2,1,0:T(8,128)(2,1)} %param.24) | copy-start | bytes 6291460
  106.2 5.5 %copy-start.14 = (bf16[16,56,2048]{2,1,0:T(8,128)(2,1)S(1)}, bf16[16,56,2048]{2,1,0:T(8,128)(2,1)}, u32[]{:S(2)}) copy-start(bf16[16,56,2048]{2,1,0:T(8,128)(2,1)} %get-tuple-element.10) | copy-start | bytes 11010052
  121.4 1.2 copy-start.3
  121.4 1.9 copy-start.6
  123.3 2.8 copy-start.9
  125.7 5.3 %collective-permute-start = (bf16[896,1024]{1,0:T(8,128)(2,1)}, bf16[896,1024]{1,0:T(8,128)(2,1)}, u32[]{:S(2)}, u32[]{:S(2)}) collective-permute-start(bf16[896,1024]{1,0:T(8,128)(2,1)} %add_convert_fusion.1), channel_id=1, source_target_pairs={{0,1},{1,0},{2,3},{3,2},{4,5},{5,4},{6,7},{7,6},{8,9},{9,8},{10,11... | collective-permute-start | bytes 5505032 | tf_op jit(solution)/shard_map/ppermute | solution.py:250
  129.9 1.2 copy-start.4
  129.9 1.9 copy-start.7
  184.4 5.1 %copy-start.12 = (f32[512]{0:T(512)S(1)}, f32[512]{0:T(512)}, u32[]{:S(2)}) copy-start(f32[512]{0:T(512)} %param.21) | copy-start | bytes 6148
  184.5 5.1 %copy-start.16 = (bf16[2048,512]{1,0:T(8,128)(2,1)S(1)}, bf16[2048,512]{1,0:T(8,128)(2,1)}, u32[]{:S(2)}) copy-start(bf16[2048,512]{1,0:T(8,128)(2,1)} %param.22) | copy-start | bytes 6291460
  189.5 1.5 copy-start.1
  189.5 6.1 %copy-start.11 = (bf16[31,512]{1,0:T(8,128)(2,1)S(1)}, bf16[31,512]{1,0:T(8,128)(2,1)}, u32[]{:S(2)}) copy-start(bf16[31,512]{1,0:T(8,128)(2,1)} %param.20) | copy-start | bytes 95236
  196.9 6.8 %copy-start.15 = (bf16[16,56,2048]{2,1,0:T(8,128)(2,1)S(1)}, bf16[16,56,2048]{2,1,0:T(8,128)(2,1)}, u32[]{:S(2)}) copy-start(bf16[16,56,2048]{2,1,0:T(8,128)(2,1)} %get-tuple-element.10) | copy-start | bytes 11010052
  203.8 4.5 %copy-start.13 = (bf16[16,56,2048]{2,1,0:T(8,128)(2,1)S(1)}, bf16[16,56,2048]{2,1,0:T(8,128)(2,1)}, u32[]{:S(2)}) copy-start(bf16[16,56,2048]{2,1,0:T(8,128)(2,1)} %get-tuple-element.9) | copy-start | bytes 11010052
  203.8 4.5 %copy-start.18 = (f32[896,512]{1,0:T(8,128)S(1)}, f32[896,512]{1,0:T(8,128)}, u32[]{:S(2)}) copy-start(f32[896,512]{1,0:T(8,128)} %fusion) | copy-start | bytes 5505028
  203.8 4.5 %copy-start.19 = (f32[896,512]{1,0:T(8,128)S(1)}, f32[896,512]{1,0:T(8,128)}, u32[]{:S(2)}) copy-start(f32[896,512]{1,0:T(8,128)} %fusion.2) | copy-start | bytes 5505028
  208.3 6.5 %copy-start.2 = (bf16[224,2048]{1,0:T(8,128)(2,1)S(1)}, bf16[224,2048]{1,0:T(8,128)(2,1)}, u32[]{:S(2)}) copy-start(bf16[224,2048]{1,0:T(8,128)(2,1)} %copy-done.1) | copy-start | bytes 2752516
  212.8 32.4 %collective-permute-start.1 = (bf16[30,512]{1,0:T(8,128)(2,1)S(1)}, bf16[30,512]{1,0:T(8,128)(2,1)S(1)}, u32[]{:S(2)}, u32[]{:S(2)}) collective-permute-start(bf16[30,512]{1,0:T(8,128)(2,1)S(1)} %slice.750), channel_id=1, source_target_pairs={{2,0},{4,2},{6,4},{8,6},{10,8},{12,10},{14,12},{16,14},{18,16},{20... | collective-permute-start | bytes 92168 | tf_op jit(solution)/shard_map/ppermute | solution.py:17
  242.9 2.3 copy-start.8
  242.9 2.3 copy-start.10
Sparse Core Ops, SparseCore 0:
  195.8 76.6 all-gather.1
where the time goes:
time: 287 us; the launch traced here: 284 us
  Pallas kernels  168 us (59%)
  matrix products  52.6 us (18%)
  waiting for transfers between devices  22.5 us (8%)
  between operations  14.3 us (5%)
  blocking collectives  8.69 us (3%)
  local copies, waits for them, and re-layouts  8.49 us (3%)
  other arithmetic  7.39 us (3%)
    pallas_call x3, Pallas kernels, exchange(): pl.pallas_call(functools.partial(exchange_body, n, number, relay, lanes),...  168 us
    all_gather x1, waiting for transfers between devices, per_device(): all_activ = lax.all_gather(activ, 'sp', axis=0, tiled=True)  22.5 us
    dot_general x5, matrix products, contract_rows(): lax.dot_general(left, right, (((0,), (0,)), ((), ())), preferred_element_...  22 us
    dot_general x5, matrix products, contract_cols(): lax.dot_general(left, right, (((1,), (1,)), ((), ())), preferred_element_...  15 us
  transfers between devices with their start and end apart: 3, of which 1 were waited for; matrix products, arithmetic and copies ran while one was open for 9% of the time, Pallas kernels for 10%

commit v1 on v0

v1 whole, which is shorter than its diff:
```python
import functools

import jax
import jax.numpy as jnp
from jax import lax
from jax.experimental import pallas as pl
from jax.experimental.pallas import tpu as pltpu
from jax.sharding import PartitionSpec as P

norm_eps = 1e-05
MESH = pl.DeviceIdType.MESH
LANES = 128
STRIP = 32


def contract_rows(left, right):
    return lax.dot_general(
        left, right, (((0,), (0,)), ((), ())), preferred_element_type=jnp.float32
    )


def contract_cols(left, right):
    return lax.dot_general(
        left, right, (((1,), (1,)), ((), ())), preferred_element_type=jnp.float32
    )


def remote(src, dst, send, recv, where):
    return pltpu.make_async_remote_copy(
        src_ref=src,
        dst_ref=dst,
        send_sem=send,
        recv_sem=recv,
        device_id=where,
        device_id_type=MESH,
    )


def signal(sem, where):
    pl.semaphore_signal(sem, inc=1, device_id=where, device_id_type=MESH)


def two_lanes(first, second):
    lane = lax.broadcasted_iota(jnp.int32, (first.shape[0], LANES), 1)
    return jnp.where(lane == 0, first, jnp.where(lane == 1, second, 0.0))


def dispatch_body(
    n, group, channels, xin, xgr, conv, gain, outs_in, outs_gr, act_out, stat_out,
    sums_mine, sums_other, act_src, own_sem, send_sem, recv_sem, fwd_send, fwd_recv,
    act_sem, act_send, act_recv, act_fsend, act_frecv, sum_sem,
):
    xs, outs = (xin, xgr), (outs_in, outs_gr)
    me, half = lax.axis_index("sp"), lax.axis_index("tp")
    other = 1 - half
    base, mine = me // group * group, lax.rem(me, group)
    rows, width = conv.shape

    def place(a, source, side):
        cols = xs[a].shape[2]
        return outs[a].at[source, :, pl.ds(pl.multiple_of(side * cols, cols), cols)]

    def act_place(source, side):
        return act_out.at[source, :, pl.ds(pl.multiple_of(side * width, width), width)]

    def outgoing(a, step):
        peer = lax.rem(me + step, n)
        return remote(
            xs[a].at[peer], place(a, me, half), send_sem.at[a, step], recv_sem.at[a, step],
            (peer, half),
        )

    def incoming(a, step):
        source = lax.rem(me + n - step, n)
        return remote(
            xs[a].at[source], place(a, source, half), send_sem.at[a, step], recv_sem.at[a, step],
            (source, half),
        )

    def relayed(a, step):
        source = lax.rem(me + n - step, n)
        return remote(
            place(a, source, half), place(a, source, half), fwd_send.at[a, step],
            fwd_recv.at[a, step], (me, other),
        )

    def first_relay(a):
        return remote(
            xs[a].at[me], place(a, me, half), fwd_send.at[a, 0], fwd_recv.at[a, 0], (me, other)
        )

    def from_other(a, step):
        source = lax.rem(me + n - step, n)
        return remote(
            xs[a].at[source], place(a, source, other), fwd_send.at[a, step],
            fwd_recv.at[a, step], (me, other),
        )

    def act_outgoing(step):
        peer = base + lax.rem(mine + step, group)
        return remote(
            act_src, act_place(mine, half), act_send.at[step], act_recv.at[step], (peer, half)
        )

    def act_incoming(step):
        source = lax.rem(mine + group - step, group)
        return remote(
            act_src, act_place(source, half), act_send.at[step], act_recv.at[step],
            (base + source, half),
        )

    def act_relayed(step):
        source = lax.rem(mine + group - step, group)
        return remote(
            act_place(source, half), act_place(source, half), act_fsend.at[step],
            act_frecv.at[step], (me, other),
        )

    def act_first():
        return remote(
            act_src, act_place(mine, half), act_fsend.at[0], act_frecv.at[0], (me, other)
        )

    def act_from_other(step):
        source = lax.rem(mine + group - step, group)
        return remote(
            act_src, act_place(source, other), act_fsend.at[step], act_frecv.at[step],
            (me, other),
        )

    def loop(first, last, body):
        def step(i, carry):
            body(i)
            return carry

        lax.fori_loop(first, last, step, 0)

    barrier = pltpu.get_barrier_semaphore()
    loop(1, n, lambda step: signal(barrier, (lax.rem(me + step, n), half)))
    signal(barrier, (me, other))
    pl.semaphore_wait(barrier, n)

    for a in range(2):
        loop(1, n, lambda step, a=a: outgoing(a, step).start())
    own = []
    for a in range(2):
        own.append(pltpu.make_async_copy(xs[a].at[me], place(a, me, half), own_sem.at[a]))
        own[-1].start()
        first_relay(a).start()

    def strip(i):
        return pl.ds(pl.multiple_of(i * STRIP, STRIP), STRIP)

    def statistics(i):
        values = conv[strip(i), :].astype(jnp.float32)
        sums_mine[strip(i), :] = two_lanes(
            jnp.sum(values, axis=1, keepdims=True),
            jnp.sum(values * values, axis=1, keepdims=True),
        )

    loop(0, rows // STRIP, statistics)
    both = remote(sums_mine, sums_other, sum_sem.at[0], sum_sem.at[1], (me, other))
    both.start()
    both.wait()

    def activate(i):
        total = sums_mine[strip(i), :] + sums_other[strip(i), :]
        center = total[:, 0:1] / channels
        spread = total[:, 1:2] / channels - center * center
        inv_std = lax.rsqrt(spread + norm_eps)
        stat_out[strip(i), :] = two_lanes(center, inv_std)
        scaled = (conv[strip(i), :].astype(jnp.float32) - center) * inv_std * gain[...]
        act_src[strip(i), :] = (scaled * jax.nn.sigmoid(scaled)).astype(jnp.bfloat16)

    loop(0, rows // STRIP, activate)
    own.append(pltpu.make_async_copy(act_src, act_place(mine, half), act_sem))
    own[-1].start()
    loop(1, group, lambda step: act_outgoing(step).start())
    act_first().start()

    def arrive(a, step):
        incoming(a, step).wait_recv()
        relayed(a, step).start()

    loop(1, n, lambda step: arrive(0, step))

    def act_arrive(step):
        act_incoming(step).wait_recv()
        act_relayed(step).start()

    loop(1, group, act_arrive)
    loop(1, n, lambda step: arrive(1, step))

    for a in range(2):

        def finish(step, a=a):
            outgoing(a, step).wait_send()
            relayed(a, step).wait_send()
            from_other(a, step).wait_recv()

        loop(1, n, finish)
        first_relay(a).wait_send()
        from_other(a, 0).wait_recv()

    def act_finish(step):
        act_outgoing(step).wait_send()
        act_relayed(step).wait_send()
        act_from_other(step).wait_recv()

    loop(1, group, act_finish)
    act_first().wait_send()
    act_from_other(0).wait_recv()
    for copy in own:
        copy.wait()


def dispatch(send_input, send_grad, conv_result, gain, group, channels, collective_id):
    n = send_input.shape[0]
    rows, width = conv_result.shape
    wide = jax.ShapeDtypeStruct(
        (n, send_input.shape[1], 2 * send_input.shape[2]), send_input.dtype
    )
    dma = pltpu.SemaphoreType.DMA
    vmem = pl.BlockSpec(memory_space=pltpu.VMEM)
    anywhere = pl.BlockSpec(memory_space=pl.ANY)
    return pl.pallas_call(
        functools.partial(dispatch_body, n, group, channels),
        out_shape=(
            wide,
            wide,
            jax.ShapeDtypeStruct((group, rows, 2 * width), jnp.bfloat16),
            jax.ShapeDtypeStruct((rows, LANES), jnp.float32),
        ),
        in_specs=[vmem] * 4,
        out_specs=(anywhere, anywhere, anywhere, vmem),
        scratch_shapes=[
            pltpu.VMEM((rows, LANES), jnp.float32),
            pltpu.VMEM((rows, LANES), jnp.float32),
            pltpu.VMEM((rows, width), jnp.bfloat16),
            dma((2,)),
            dma((2, n)),
            dma((2, n)),
            dma((2, n)),
            dma((2, n)),
            dma,
            dma((group,)),
            dma((group,)),
            dma((group,)),
            dma((group,)),
            dma((2,)),
        ],
        compiler_params=pltpu.CompilerParams(collective_id=collective_id, has_side_effects=True),
    )(send_input, send_grad, conv_result, gain)


def giveback_body(n, x, out, own_sem, send_sem, recv_sem):
    me, half = lax.axis_index("sp"), lax.axis_index("tp")

    def outgoing(step):
        peer = lax.rem(me + step, n)
        return remote(
            x.at[peer], out.at[me], send_sem.at[step], recv_sem.at[step], (peer, half)
        )

    def incoming(step):
        source = lax.rem(me + n - step, n)
        return remote(
            x.at[source], out.at[source], send_sem.at[step], recv_sem.at[step], (source, half)
        )

    barrier = pltpu.get_barrier_semaphore()

    def loop(body):
        def step(i, carry):
            body(i)
            return carry

        lax.fori_loop(1, n, step, 0)

    loop(lambda step: signal(barrier, (lax.rem(me + step, n), half)))
    pl.semaphore_wait(barrier, n - 1)
    loop(lambda step: outgoing(step).start())
    own = pltpu.make_async_copy(x.at[me], out.at[me], own_sem)
    own.start()

    def finish(step):
        incoming(step).wait_recv()
        outgoing(step).wait_send()

    loop(finish)
    own.wait()


def giveback(x, collective_id):
    n = x.shape[0]
    dma = pltpu.SemaphoreType.DMA
    return pl.pallas_call(
        functools.partial(giveback_body, n),
        out_shape=jax.ShapeDtypeStruct(x.shape, x.dtype),
        in_specs=[pl.BlockSpec(memory_space=pltpu.VMEM)],
        out_specs=pl.BlockSpec(memory_space=pltpu.VMEM),
        scratch_shapes=[dma, dma((n,)), dma((n,))],
        compiler_params=pltpu.CompilerParams(collective_id=collective_id, has_side_effects=True),
    )(x)


def tail_body(
    n, group, reach, token_scale, channels,
    share, feats, act, proj_w, conv, stat, gain, taps, value, gate,
    igrad, pgrad, vgrad, ggrad,
    feat_buf, sums_mine, sums_other, ext, halo_src, halo_buf, piece, rs_buf,
    local_sem, pair_sem, feat_send, feat_recv, piece_send, piece_recv, halo_sem,
):
    me, half = lax.axis_index("sp"), lax.axis_index("tp")
    other = 1 - half
    mine, my_group = lax.rem(me, group), me // group
    base = my_group * group
    groups = n // group
    per_half = groups // 2
    rows, share_width = share.shape
    width = conv.shape[1]
    piece_rows = feats.shape[2] // per_half
    rim = halo_src.shape[0]
    last = n - 1

    def loop(first, end, body):
        def step(i, carry):
            body(i)
            return carry

        lax.fori_loop(first, end, step, 0)

    def strip(i):
        return pl.ds(pl.multiple_of(i * STRIP, STRIP), STRIP)

    barrier = pltpu.get_barrier_semaphore()
    signal(barrier, (me, other))
    for step in range(1, group):
        signal(barrier, (base + lax.rem(mine + step, group), half))
    for step in range(1, groups):
        for side in range(2):
            signal(barrier, (lax.rem(my_group + step, groups) * group + mine, side))

    @pl.when(me > 0)
    def _():
        signal(barrier, (me - 1, half))

    @pl.when(me < last)
    def _():
        signal(barrier, (me + 1, half))

    ends = jnp.where(me > 0, 1, 0) + jnp.where(me < last, 1, 0)
    pl.semaphore_wait(barrier, 1 + (group - 1) + 2 * (groups - 1) + ends)

    def side_cols(side):
        return pl.ds(pl.multiple_of(side * share_width, share_width), share_width)

    to_pair = remote(
        share, igrad.at[:, side_cols(half)], pair_sem.at[0], pair_sem.at[1], (me, other)
    )
    to_pair.start()
    keep = pltpu.make_async_copy(share, igrad.at[:, side_cols(half)], local_sem.at[0])
    keep.start()

    def feat_out(step):
        peer = lax.rem(mine + step, group)
        return remote(
            feats.at[peer], feat_buf.at[mine], feat_send.at[step], feat_recv.at[step],
            (base + peer, half),
        )

    def feat_in(step):
        source = lax.rem(mine + group - step, group)
        return remote(
            feats.at[source], feat_buf.at[source], feat_send.at[step], feat_recv.at[step],
            (base + source, half),
        )

    for step in range(1, group):
        feat_out(step).start()
    keep_feat = pltpu.make_async_copy(feats.at[mine], feat_buf.at[mine], local_sem.at[1])
    keep_feat.start()

    keep.wait()
    to_pair.wait()
    ext[0:rows, :] = jnp.dot(igrad[...], proj_w[...], preferred_element_type=jnp.float32)

    def normed_of(i):
        center, inv_std = stat[strip(i), 0:1], stat[strip(i), 1:2]
        return (conv[strip(i), :].astype(jnp.float32) - center) * inv_std, inv_std

    def norm_back(i):
        normed, _ = normed_of(i)
        scaled = normed * gain[...]
        sig = jax.nn.sigmoid(scaled)
        back = ext[strip(i), :] * sig * (1.0 + scaled * (1.0 - sig)) * gain[...]
        ext[strip(i), :] = back
        sums_mine[strip(i), :] = two_lanes(
            jnp.sum(back, axis=1, keepdims=True), jnp.sum(back * normed, axis=1, keepdims=True)
        )

    loop(0, rows // STRIP, norm_back)
    sums = remote(sums_mine, sums_other, pair_sem.at[2], pair_sem.at[3], (me, other))
    sums.start()

    keep_feat.wait()
    for step in range(1, group):
        feat_in(step).wait_recv()
    received = feat_buf[...].reshape(group * rows, feats.shape[2])

    def piece_out(q, side, where):
        return remote(
            piece.at[q, side], rs_buf.at[my_group], piece_send.at[q, side],
            piece_recv.at[my_group], (where * group + mine, side),
        )

    def piece_keep(q, side):
        return pltpu.make_async_copy(piece.at[q, side], rs_buf.at[my_group], local_sem.at[2])

    def each_piece(sides, at_home, away):
        for side in sides:
            for q in range(per_half):
                where = half * per_half + q
                home = jnp.logical_and(where == my_group, half == side)

                @pl.when(home)
                def _(q=q, side=side):
                    at_home(q, side)

                @pl.when(jnp.logical_not(home))
                def _(q=q, side=side, where=where):
                    away(q, side, where)

    for side in range(2):
        partial = contract_rows(
            received, act[:, side * width : (side + 1) * width]
        ).astype(jnp.bfloat16)
        for q in range(per_half):
            piece[q, side] = partial[q * piece_rows : (q + 1) * piece_rows]
    each_piece(
        range(2),
        lambda q, side: piece_keep(q, side).start(),
        lambda q, side, where: piece_out(q, side, where).start(),
    )

    sums.wait()

    def conv_back(i):
        normed, inv_std = normed_of(i)
        total = (sums_mine[strip(i), :] + sums_other[strip(i), :]) / channels
        ext[strip(i), :] = inv_std * (
            ext[strip(i), :] - total[:, 0:1] - normed * total[:, 1:2]
        )

    loop(0, rows // STRIP, conv_back)
    halo_src[...] = ext[0:rim, :].astype(jnp.bfloat16)

    def halo_copy(where):
        return remote(halo_src, halo_buf, halo_sem.at[0], halo_sem.at[1], (where, half))

    @pl.when(me > 0)
    def _():
        halo_copy(me - 1).start()

    @pl.when(me < last)
    def _():
        halo_copy(me + 1).wait_recv()
        ext[rows : rows + rim, :] = halo_buf[...].astype(jnp.float32)

    @pl.when(me == last)
    def _():
        ext[rows : rows + rim, :] = jnp.zeros((rim, width), jnp.float32)

    def convolve(c):
        cols = pl.ds(pl.multiple_of(c * LANES, LANES), LANES)
        mixed = jnp.zeros((rows, LANES), jnp.float32)
        for lag in range(reach):
            tap = taps[reach - 1 - lag : reach - lag, cols]
            mixed = mixed + tap * ext[lag : lag + rows, cols]
        sig = jax.nn.sigmoid(gate[:, cols].astype(jnp.float32))
        vgrad[:, cols] = (mixed * sig).astype(jnp.bfloat16)
        ggrad[:, cols] = (
            mixed * value[:, cols].astype(jnp.float32) * sig * (1.0 - sig)
        ).astype(jnp.bfloat16)

    loop(0, width // LANES, convolve)

    def piece_in(source):
        return remote(
            piece.at[0, 0], rs_buf.at[source], piece_send.at[0, 0], piece_recv.at[source],
            (source * group + mine, half),
        )

    my_half = my_group // per_half
    for source in range(groups):

        @pl.when(jnp.logical_not(jnp.logical_and(source == my_group, half == my_half)))
        def _(source=source):
            piece_in(source).wait_recv()

    each_piece(
        range(2),
        lambda q, side: piece_keep(q, side).wait(),
        lambda q, side, where: piece_out(q, side, where).wait_send(),
    )
    total = rs_buf[0].astype(jnp.float32)
    for source in range(1, groups):
        total = total + rs_buf[source].astype(jnp.float32)
    pgrad[...] = total * token_scale

    for step in range(1, group):
        feat_out(step).wait_send()

    @pl.when(me > 0)
    def _():
        halo_copy(me - 1).wait_send()


def tail(
    share, feats, act, proj_w, conv, stat, gain, taps, value, gate, n, token_scale, channels,
    collective_id,
):
    group, rows, wide = feats.shape
    width = conv.shape[1]
    groups = n // group
    per_half = groups // 2
    piece_rows = wide // per_half
    reach = taps.shape[0]
    rim = -(-(reach - 1) // 16) * 16
    dma = pltpu.SemaphoreType.DMA
    vmem = pl.BlockSpec(memory_space=pltpu.VMEM)
    return pl.pallas_call(
        functools.partial(tail_body, n, group, reach, token_scale, channels),
        out_shape=(
            jax.ShapeDtypeStruct((rows, 2 * share.shape[1]), jnp.bfloat16),
            jax.ShapeDtypeStruct((piece_rows, width), jnp.float32),
            jax.ShapeDtypeStruct((rows, width), jnp.bfloat16),
            jax.ShapeDtypeStruct((rows, width), jnp.bfloat16),
        ),
        in_specs=[vmem] * 10,
        out_specs=(vmem,) * 4,
        scratch_shapes=[
            pltpu.VMEM((group, rows, wide), jnp.bfloat16),
            pltpu.VMEM((rows, LANES), jnp.float32),
            pltpu.VMEM((rows, LANES), jnp.float32),
            pltpu.VMEM((rows + rim, width), jnp.float32),
            pltpu.VMEM((rim, width), jnp.bfloat16),
            pltpu.VMEM((rim, width), jnp.bfloat16),
            pltpu.VMEM((per_half, 2, piece_rows, width), jnp.bfloat16),
            pltpu.VMEM((groups, piece_rows, width), jnp.bfloat16),
            dma((3,)),
            dma((4,)),
            dma((group,)),
            dma((group,)),
            dma((per_half, 2)),
            dma((groups,)),
            dma((2,)),
        ],
        compiler_params=pltpu.CompilerParams(collective_id=collective_id, has_side_effects=True),
    )(share, feats, act, proj_w, conv, stat, gain, taps, value, gate)


def per_device(
    out_grad,
    moe_input,
    routes,
    route_weights,
    conv_result,
    glu_value,
    glu_gate,
    conv_taps,
    norm_gain,
    proj_weight,
    expert_gate,
    expert_up,
    expert_down,
):
    n_sp = lax.axis_size("sp")
    n_tp = lax.axis_size("tp")
    half = lax.axis_index("tp")
    tok_rows, width = out_grad.shape
    top_count = routes.shape[1]
    bound = 2 * top_count * tok_rows // n_sp
    capacity = -(-bound // 8) * 8
    slots = n_sp * capacity
    share = width // n_tp
    channels = conv_result.shape[1] * n_tp
    group = n_sp // 4
    gain = norm_gain[None, :]
    experts = jnp.arange(n_sp, dtype=jnp.int32)[None, :]
    named = [(routes[:, k : k + 1] == experts) for k in range(top_count)]
    per_token = sum(hit.astype(jnp.bfloat16) for hit in named)
    order = jnp.arange(tok_rows, dtype=jnp.int32)
    before = (order[None, :] < order[:, None]).astype(jnp.bfloat16)
    earlier = jnp.dot(before, per_token, preferred_element_type=jnp.float32).astype(jnp.int32)
    rows = jnp.arange(slots, dtype=jnp.int32)
    chosen = []
    for k in range(top_count):
        slot = jnp.sum(jnp.where(named[k], earlier, 0), axis=1)
        target = routes[:, k] * capacity + slot
        chosen.append(rows[:, None] == target[None, :])
    pick = functools.reduce(jnp.logical_or, chosen).astype(jnp.bfloat16)
    row_weight = sum(
        jnp.sum(jnp.where(chosen[k], route_weights[:, k][None, :], 0.0), axis=1)
        for k in range(top_count)
    )
    input_half = lax.dynamic_slice_in_dim(moe_input, half * share, share, 1)
    grad_half = lax.dynamic_slice_in_dim(out_grad, half * share, share, 1)
    send_input = jnp.dot(pick, input_half, preferred_element_type=jnp.float32).astype(jnp.bfloat16)
    send_grad = (
        jnp.dot(pick, grad_half, preferred_element_type=jnp.float32) * row_weight[:, None]
    ).astype(jnp.bfloat16)
    row_scale = float(n_sp * bound) ** (-0.5)
    blocks = (n_sp, capacity, share)
    inputs, grads, all_act, stat = dispatch(
        send_input.reshape(blocks), send_grad.reshape(blocks), conv_result, gain, group,
        channels, 1,
    )
    inputs, grads = inputs.reshape(slots, width), grads.reshape(slots, width)

    gate_pre = jnp.dot(inputs, expert_gate[0], preferred_element_type=jnp.float32)
    up_pre = jnp.dot(inputs, expert_up[0], preferred_element_type=jnp.float32)
    sigma = jax.nn.sigmoid(gate_pre)
    silu_gate = gate_pre * sigma
    hidden = (silu_gate * up_pre).astype(jnp.bfloat16)
    down_g = contract_rows(hidden, grads) * row_scale
    hidden_grad = contract_cols(grads, expert_down[0])
    gate_back = (hidden_grad * up_pre * sigma * (1.0 + gate_pre * (1.0 - sigma))).astype(
        jnp.bfloat16
    )
    up_back = (hidden_grad * silu_gate).astype(jnp.bfloat16)
    gate_g = contract_rows(inputs, gate_back) * row_scale
    up_g = contract_rows(inputs, up_back) * row_scale

    def partial_of(side):
        weight_g = lax.dynamic_slice_in_dim(expert_gate[0], side * share, share, 0)
        weight_u = lax.dynamic_slice_in_dim(expert_up[0], side * share, share, 0)
        return (contract_cols(gate_back, weight_g) + contract_cols(up_back, weight_u)).astype(
            jnp.bfloat16
        )

    arrived = lax.ppermute(
        partial_of(1 - half), "tp", [(i, n_tp - 1 - i) for i in range(n_tp)]
    )
    summed = (partial_of(half).astype(jnp.float32) + arrived.astype(jnp.float32)).astype(
        jnp.bfloat16
    )
    returned = giveback(summed.reshape(blocks), 2).reshape(slots, share)
    grad_share = (grad_half.astype(jnp.float32) + contract_rows(pick, returned)).astype(
        jnp.bfloat16
    )
    groups = n_sp // group
    feature = width // n_sp
    per_half = groups // n_tp
    feats = (
        grad_share.reshape(tok_rows, per_half, group, feature)
        .transpose(2, 0, 1, 3)
        .reshape(group, tok_rows, per_half * feature)
    )
    input_grad, proj_grad, value_grad, gate_side_grad = tail(
        grad_share, feats, all_act.reshape(group * tok_rows, channels), proj_weight,
        conv_result, stat, gain, conv_taps.astype(jnp.float32), glu_value, glu_gate, n_sp,
        float(tok_rows * n_sp) ** (-0.5), channels, 3,
    )
    return (
        input_grad,
        proj_grad,
        gate_g[None],
        up_g[None],
        down_g[None],
        value_grad,
        gate_side_grad,
    )


def solution(mesh):
    in_specs = (
        P("sp", None),
        P("sp", None),
        P("sp", None),
        P("sp", None),
        P("sp", "tp"),
        P("sp", "tp"),
        P("sp", "tp"),
        P(None, "tp"),
        P("tp"),
        P(None, "tp"),
        P("sp", None, "tp"),
        P("sp", None, "tp"),
        P("sp", "tp", None),
    )
    out_specs = (
        P("sp", None),
        P("sp", "tp"),
        P("sp", None, "tp"),
        P("sp", None, "tp"),
        P("sp", "tp", None),
        P("sp", "tp"),
        P("sp", "tp"),
    )
    return jax.shard_map(
        per_device, mesh=mesh, in_specs=in_specs, out_specs=out_specs, check_vma=False
    )
```

time: 287 us -> 225 us (0.78)
  waiting for transfers between devices: 22.5 us -> 0.01 us
  between operations: 14.3 us -> 0.85 us
  matrix products: 52.6 us -> 42 us
  blocking collectives: 8.69 us -> 0 us
  other arithmetic: 7.39 us -> 0.96 us
  Pallas kernels: 168 us -> 171 us
    all_gather x1 -> x0, waiting for transfers between devices: 22.5 us -> none  [per_device(): all_activ = lax.all_gather(activ, 'sp', axis=0, tiled=True)]
    dot_general x5 -> x4, matrix products: 22 us -> 15.7 us  [contract_rows(): lax.dot_general(left, right, (((0,), (0,)), ((), ())), preferred_element_...]
    psum x2 -> x0, blocking collectives: 6.05 us -> none  [the longest x1 3.6 us: per_device(): lax.psum((jnp.sum(values, axis=1), jnp.sum(values * values, axis=1)), 'tp')]
    convert_element_type x3 -> x1, other arithmetic: 4.79 us -> 0.64 us  [per_device(): conv_taps.astype(jnp.float32)]
    pallas_call x3, Pallas kernels: 168 us -> 171 us  [the longest x1 92.9 us: dispatch(): pl.pallas_call(functools.partial(dispatch_body, n, group, channels), out_...]
    unnamed x41 -> x30, local copies, waits for them, and re-layouts: 2.46 us -> 5.79 us
    transpose x2 -> x0, local copies, waits for them, and re-layouts: 3.07 us -> none  [the longest x1 2.21 us: per_device(): features.transpose(1, 0, 2, 3).reshape(n_sp * tok_rows, width // n_sp)]
  transfers between devices with their start and end apart: 3 -> 1, of which waited for: 1 -> 0; matrix products, arithmetic and copies ran while one was open for 9% -> 7% of each run, Pallas kernels for 10% -> 0%
where the time goes in v1:
time: 225 us
  Pallas kernels  171 us (76%)
  matrix products  42 us (19%)
  local copies, waits for them, and re-layouts  9.16 us (4%)
    pallas_call x1, Pallas kernels, dispatch(): pl.pallas_call(functools.partial(dispatch_body, n, group, channels), out_...  92.9 us
    pallas_call x1, Pallas kernels, giveback(): pl.pallas_call(functools.partial(giveback_body, n), out_shape=jax.ShapeDt...  49.4 us
    pallas_call x1, Pallas kernels, tail(): pl.pallas_call(functools.partial(tail_body, n, group, reach, token_scale,...  28.9 us
    dot_general x4, matrix products, contract_rows(): lax.dot_general(left, right, (((0,), (0,)), ((), ())), preferred_element_...  15.7 us
    dot_general x5, matrix products, contract_cols(): lax.dot_general(left, right, (((1,), (1,)), ((), ())), preferred_element_...  12.3 us
    unnamed x30, local copies, waits for them, and re-layouts  5.79 us
    dot_general x1, matrix products, per_device(): jnp.dot(inputs, expert_gate[0], preferred_element_type=jnp.float32)  5.48 us
  transfers between devices with their start and end apart: 1, of which 0 were waited for; matrix products, arithmetic and copies ran while one was open for 7% of the time, Pallas kernels for 0%

profile of v1, /device:TPU:14, one launch (start us, length us, event | category | flops | bytes accessed | tf_op | source)
XLA Modules:
  0.0 224.6 jit_solution(15491015776103076023)
XLA Ops:
  0.7 0.9 fusion.46
  1.5 0.8 fusion.45
  2.8 3.0 %convolution_convert_fusion = bf16[896,1024]{1,0:T(8,128)(2,1)} fusion(bf16[224,2048]{1,0:T(8,128)(2,1)} %param.14, s32[]{:T(128)S(6)} %select_n.24, s32[224]{0:T(256)S(1)} %get-tuple-element.31, s32[224]{0:T(256)S(1)} %get-tuple-element.32), kind=kOutput, calls=%fused_computation.18 | convolution fusion | flops 412561408 | bytes 2295556 | tf_op jit(solution)/shard_map/dot_general | solution.py:609
  5.9 2.0 multiply_convert_fusion
  7.9 92.9 %shard_map.180 = (bf16[16,56,2048]{2,1,0:T(8,128)(2,1)}, bf16[16,56,2048]{2,1,0:T(8,128)(2,1)}, bf16[4,224,1024]{2,1,0:T(8,128)(2,1)}, f32[224,128]{1,0:T(8,128)}) custom-call(bf16[16,56,1024]{2,1,0:T(8,128)(2,1)} %bitcast.58, bf16[16,56,1024]{2,1,0:T(8,128)(2,1)} %bitcast.59, bf16[224,512]{1,0:T(8,128)(2,1)} %conv.3, f32[1,512]{1,0:T(1,128)} %bitcast.63), custom_call_target="tpu_custom_call" | custom-call | tf_op jit(solution)/shard_map/pallas_call | solution.py:226
  100.8 5.5 %fusion = f32[896,512]{1,0:T(8,128)} fusion(bf16[896,2048]{1,0:T(8,128)(2,1)} %bitcast.73, bf16[1,2048,512]{2,1,0:T(8,128)(2,1)S(1)} %copy-done), kind=kOutput, calls=%fused_computation.7 | convolution fusion | flops 1879048192 | bytes 7602176 | tf_op jit(solution)/shard_map/dot_general | solution.py:621
  106.3 3.3 %fusion.2 = f32[896,512]{1,0:T(8,128)} fusion(bf16[896,2048]{1,0:T(8,128)(2,1)S(1)} %bitcast.74, bf16[1,2048,512]{2,1,0:T(8,128)(2,1)S(1)} %copy-done.1), kind=kOutput, calls=%fused_computation.9 | convolution fusion | flops 1879048192 | bytes 7602176 | tf_op jit(solution)/shard_map/dot_general | solution.py:622
  109.6 6.4 %multiply_convert_fusion.2 = (bf16[896,512]{1,0:T(8,128)(2,1)S(1)}, bf16[896,512]{1,0:T(8,128)(2,1)S(1)}) fusion(f32[896,512]{1,0:T(8,128)} %fusion, f32[896,512]{1,0:T(8,128)} %fusion.2, bf16[896,2048]{1,0:T(8,128)(2,1)} %bitcast.71, bf16[1,512,2048]{2,1,0:T(8,128)(2,1)} %param.25), kind=kOutput, calls=%fused_computation.14 | convolution fusion | flops 1885011968 | bytes 11272192 | tf_op jit(solution)/shard_map/dot_general | solution.py:23
  116.0 1.2 fusion.9
  117.6 1.2 add_convert_fusion.1
  119.2 1.1 fusion.12
  120.4 0.6 convert_element_type.64.taps
  121.0 4.4 %multiply_bitcast_fusion.1 = f32[1,2048,512]{2,1,0:T(8,128)} fusion(bf16[896,2048]{1,0:T(8,128)(2,1)S(1)} %bitcast.75, bf16[896,512]{1,0:T(8,128)(2,1)S(1)} %get-tuple-element.25), kind=kOutput, calls=%fused_computation.1 | convolution fusion | flops 1880096768 | bytes 8781824 | tf_op jit(solution)/shard_map/dot_general | solution.py:17
  125.4 4.6 %multiply_bitcast_fusion.2 = f32[1,2048,512]{2,1,0:T(8,128)} fusion(bf16[896,2048]{1,0:T(8,128)(2,1)S(1)} %bitcast.76, bf16[896,512]{1,0:T(8,128)(2,1)S(1)} %get-tuple-element.26), kind=kOutput, calls=%fused_computation.2 | convolution fusion | flops 1880096768 | bytes 8781824 | tf_op jit(solution)/shard_map/dot_general | solution.py:17
  130.0 4.5 %multiply_bitcast_fusion = f32[1,512,2048]{2,1,0:T(8,128)} fusion(bf16[896,2048]{1,0:T(8,128)(2,1)S(1)} %bitcast.72, f32[896,512]{1,0:T(8,128)S(1)} %copy-done.12, f32[896,512]{1,0:T(8,128)S(1)} %copy-done.11), kind=kOutput, calls=%fused_computation | convolution fusion | flops 1882849280 | bytes 11534336 | tf_op jit(solution)/shard_map/dot_general | solution.py:17
  134.5 2.4 %add_convert_fusion = bf16[896,1024]{1,0:T(8,128)(2,1)} fusion(bf16[896,1024]{1,0:T(8,128)(2,1)S(1)} %collective-permute-done, f32[896,1024]{1,0:T(8,128)S(1)} %fusion.12, bf16[896,512]{1,0:T(8,128)(2,1)S(1)} %get-tuple-element.25, bf16[1,2048,512]{2,1,0:T(8,128)(2,1)S(1)} %copy-done.2, s32[]{:T(128)S(6)} %select_n.24), kind=kOutput, calls=%fused_computation.3 | convolution fusion | flops 945029120 | bytes 9306116 | tf_op jit(solution)/shard_map/dot_general | solution.py:23
  136.9 49.4 %shard_map.181 = bf16[16,56,1024]{2,1,0:T(8,128)(2,1)} custom-call(bf16[16,56,1024]{2,1,0:T(8,128)(2,1)} %bitcast.57), custom_call_target="tpu_custom_call" | custom-call | tf_op jit(solution)/shard_map/pallas_call | solution.py:297
  186.4 2.2 fusion.7.share
  189.3 1.1 reshape.75.feats
  190.4 28.9 %shard_map.182 = (bf16[224,2048]{1,0:T(8,128)(2,1)}, f32[128,512]{1,0:T(8,128)}, bf16[224,512]{1,0:T(8,128)(2,1)}, bf16[224,512]{1,0:T(8,128)(2,1)}) custom-call(bf16[224,1024]{1,0:T(8,128)(2,1)} %copy-done.3, bf16[4,224,256]{2,1,0:T(8,128)(2,1)} %reshape.75.feats, bf16[896,1024]{1,0:T(8,128)(2,1)} %bitcast.62, bf16[2048,512]{1,0:T(8,128)(2,1)} %proj_w.1, ...), custom_call_target="tpu_custom_call" | custom-call | tf_op jit(solution)/shard_map/pallas_call | solution.py:532
  219.3 2.3 %copy.28 = bf16[224,2048]{1,0:T(8,128)(2,1)} copy(bf16[224,2048]{1,0:T(8,128)(2,1)} %get-tuple-element.40) | data formatting | bytes 1835008
  221.5 1.7 copy.29
  223.2 0.7 copy.30
  223.9 0.7 copy.31
  (35 shorter events, 2.1 us)
Async XLA Ops:
  0.6 100.2 %copy-start = (bf16[1,2048,512]{2,1,0:T(8,128)(2,1)S(1)}, bf16[1,2048,512]{2,1,0:T(8,128)(2,1)}, u32[]{:S(2)}) copy-start(bf16[1,2048,512]{2,1,0:T(8,128)(2,1)} %param.23) | copy-start | bytes 6291460
  0.6 5.2 %copy-start.10 = (bf16[224,2048]{1,0:T(8,128)(2,1)S(1)}, bf16[224,2048]{1,0:T(8,128)(2,1)}, u32[]{:S(2)}) copy-start(bf16[224,2048]{1,0:T(8,128)(2,1)} %param.13) | copy-start | bytes 2752516
  100.8 5.5 %copy-start.1 = (bf16[1,2048,512]{2,1,0:T(8,128)(2,1)S(1)}, bf16[1,2048,512]{2,1,0:T(8,128)(2,1)}, u32[]{:S(2)}) copy-start(bf16[1,2048,512]{2,1,0:T(8,128)(2,1)} %param.24) | copy-start | bytes 6291460
  100.8 5.5 %copy-start.8 = (bf16[16,56,2048]{2,1,0:T(8,128)(2,1)S(1)}, bf16[16,56,2048]{2,1,0:T(8,128)(2,1)}, u32[]{:S(2)}) copy-start(bf16[16,56,2048]{2,1,0:T(8,128)(2,1)} %get-tuple-element.16) | copy-start | bytes 11010052
  116.0 1.6 copy-start.2
  118.7 1.6 copy-start.6
  118.8 2.2 copy-start.9
  118.8 15.8 %collective-permute-start = (bf16[896,1024]{1,0:T(8,128)(2,1)S(1)}, bf16[896,1024]{1,0:T(8,128)(2,1)S(1)}, u32[]{:S(2)}, u32[]{:S(2)}) collective-permute-start(bf16[896,1024]{1,0:T(8,128)(2,1)S(1)} %add_convert_fusion.1), channel_id=1, source_target_pairs={{0,1},{1,0},{2,3},{3,2},{4,5},{5,4},{6,7},{7,6},{8,9},{9,8},{10,11... | collective-permute-start | bytes 5505032 | tf_op jit(solution)/shard_map/ppermute | solution.py:642
  125.4 4.6 %copy-start.7 = (bf16[16,56,2048]{2,1,0:T(8,128)(2,1)S(1)}, bf16[16,56,2048]{2,1,0:T(8,128)(2,1)}, u32[]{:S(2)}) copy-start(bf16[16,56,2048]{2,1,0:T(8,128)(2,1)} %get-tuple-element.15) | copy-start | bytes 11010052
  125.4 4.6 %copy-start.11 = (f32[896,512]{1,0:T(8,128)S(1)}, f32[896,512]{1,0:T(8,128)}, u32[]{:S(2)}) copy-start(f32[896,512]{1,0:T(8,128)} %fusion) | copy-start | bytes 5505028
  125.4 4.6 %copy-start.12 = (f32[896,512]{1,0:T(8,128)S(1)}, f32[896,512]{1,0:T(8,128)}, u32[]{:S(2)}) copy-start(f32[896,512]{1,0:T(8,128)} %fusion.2) | copy-start | bytes 5505028
  188.6 1.8 copy-start.3
  219.3 3.9 %copy-start.5 = (bf16[224,512]{1,0:T(8,128)(2,1)S(1)}, bf16[224,512]{1,0:T(8,128)(2,1)}, u32[]{:S(2)}) copy-start(bf16[224,512]{1,0:T(8,128)(2,1)} %get-tuple-element.45) | copy-start | bytes 688132
  219.3 4.6 %copy-start.4 = (bf16[224,512]{1,0:T(8,128)(2,1)S(1)}, bf16[224,512]{1,0:T(8,128)(2,1)}, u32[]{:S(2)}) copy-start(bf16[224,512]{1,0:T(8,128)(2,1)} %get-tuple-element.46) | copy-start | bytes 688132
